TPU v7x, 32 devices: a whole 2x2x4 slice. The times are simulated.
32 devices in a mesh: sp: 8 (over z, y), tp: 4 (over x, core).
Axes of the slice: x: 2, y: 2, z: 4, core: 2. Of those that a mesh axis runs over, the one named last changes fastest.
Arguments:
- inputs: bfloat16 [8192, 2048], P('sp'), may hold values from -6 to 6
- norm_gain: float32 [3, 2048], replicated, may hold values from 0.1 to 1.9
- query_weight: bfloat16 [3, 2048, 1024], P(None, 'sp', 'tp'), may hold values from -64 to 64
- key_weight: bfloat16 [3, 2048, 512], P(None, 'sp', 'tp'), may hold values from -4 to 4
- value_weight: bfloat16 [3, 2048, 512], P(None, 'sp', 'tp'), may hold values from -0.125 to 0.125
- output_weight: bfloat16 [3, 2048, 1024], P(None, 'sp', 'tp'), may hold values from -0.1875 to 0.1875
- sink_logit: float32 [3, 16], P(None, 'tp'), may hold values from 2 to 7
- final_gain: float32 [2048], replicated, may hold values from 0.1 to 1.9
Outputs:
- result: float32 [8192, 2048], P(('sp', 'tp'))
All inputs are finite; a program needn't handle non-finite values.
Results may differ from a plain program's by a relative error of at most 0.015.
Values may be sent and summed in bfloat16 or wider, within the bound.
A program may use at most 64 MiB of HBM per device.

v0:
```python
import jax
import jax.numpy as jnp
from jax import lax
from jax.sharding import PartitionSpec as P

D = 2048
HEAD_DIM = 64
WINDOW = 128
LAYERS = 3
EPS = 1e-06


def extended_2(block, sides, width):
    for axis, dim in sides:
        count = lax.axis_size(axis)
        forward = [(i, i + 1) for i in range(count - 1)]
        backward = [(target, source) for source, target in forward]
        low = lax.ppermute(
            lax.slice_in_dim(block, block.shape[dim] - width, None, axis=dim), axis, forward
        )
        high = lax.ppermute(lax.slice_in_dim(block, 0, width, axis=dim), axis, backward)
        block = jnp.concatenate([low, block, high], axis=dim)
    return block


def norm_rows(values, gain):
    wide_values = values.astype(jnp.float32)
    inv_root = lax.rsqrt(jnp.mean(wide_values * wide_values, axis=-1, keepdims=True) + EPS)
    return wide_values * inv_root * gain


def rotate(values, places):
    half_dim = values.shape[-1] // 2
    inverse = 10000.0 ** (-jnp.arange(half_dim).astype(jnp.float32) / half_dim)
    angles = places[:, None] * inverse[None, :]
    cosine_table = jnp.cos(angles)[:, None, :]
    sine_table = jnp.sin(angles)[:, None, :]
    front_half = values[..., :half_dim]
    back_half = values[..., half_dim:]
    return jnp.concatenate(
        [
            front_half * cosine_table - back_half * sine_table,
            back_half * cosine_table + front_half * sine_table,
        ],
        axis=-1,
    )


def attend(queries, key_rows, value_rows, sink_row, allowed):
    scores = jnp.einsum(
        "qkgd,skd->kgqs", queries, key_rows, preferred_element_type=jnp.float32
    ) * queries.shape[-1] ** (-0.5)
    scores = jnp.where(allowed[None, None], scores, -jnp.inf)
    sink_col = sink_row[:, :, None]
    largest = jnp.maximum(jnp.max(scores, axis=-1), sink_col)
    powers = jnp.exp(scores - largest[..., None])
    denominator = jnp.sum(powers, axis=-1) + jnp.exp(sink_col - largest)
    weights = (powers / denominator[..., None]).astype(jnp.bfloat16)
    blended = jnp.einsum("kgqs,skd->qkgd", weights, value_rows, preferred_element_type=jnp.float32)
    return blended.astype(jnp.bfloat16)


def shards(
    inputs, norm_gain, query_weight, key_weight, value_weight, output_weight, sink_logit, final_gain
):
    tokens = inputs.shape[0]
    local_heads = query_weight.shape[2] // HEAD_DIM
    local_groups = key_weight.shape[2] // HEAD_DIM
    per_group = local_heads // local_groups
    kv_cols = local_groups * HEAD_DIM
    offset = lax.axis_index("sp") * tokens
    seq_total = tokens * lax.axis_size("sp")
    query_pos = offset + jnp.arange(tokens, dtype=jnp.int32)
    places = query_pos.astype(jnp.float32)
    key_pos = offset - WINDOW + jnp.arange(tokens + 2 * WINDOW, dtype=jnp.int32)
    allowed = (
        (jnp.abs(key_pos[None, :] - query_pos[:, None]) <= WINDOW)
        & (key_pos[None, :] >= 0)
        & (key_pos[None, :] < seq_total)
    )
    whole_query, whole_key, whole_value, whole_out = (
        lax.all_gather(query_weight, "sp", axis=1, tiled=True),
        lax.all_gather(key_weight, "sp", axis=1, tiled=True),
        lax.all_gather(value_weight, "sp", axis=1, tiled=True),
        lax.all_gather(output_weight, "sp", axis=1, tiled=True),
    )
    current = inputs
    final_rows = inputs
    for layer in range(LAYERS):
        normed = norm_rows(current, norm_gain[layer]).astype(jnp.bfloat16)
        query_raw = jnp.dot(normed, whole_query[layer], preferred_element_type=jnp.float32)
        key_raw = jnp.dot(normed, whole_key[layer], preferred_element_type=jnp.float32)
        value_raw = jnp.dot(normed, whole_value[layer], preferred_element_type=jnp.float32)
        out_weight = whole_out[layer]
        queries = rotate(
            (query_raw * float(D) ** (-0.5)).reshape(tokens, local_heads, HEAD_DIM), places
        ).astype(jnp.bfloat16)
        key_rot = rotate(
            (key_raw * float(D) ** (-0.5)).reshape(tokens, local_groups, HEAD_DIM), places
        ).astype(jnp.bfloat16)
        packed = jnp.concatenate(
            [key_rot.reshape(tokens, kv_cols), value_raw.astype(jnp.bfloat16)], axis=1
        )
        extended = extended_2(packed, (("sp", 0),), WINDOW)
        key_rows = extended[:, :kv_cols].reshape(-1, local_groups, HEAD_DIM)
        value_all = extended[:, kv_cols:].reshape(-1, local_groups, HEAD_DIM)
        sink_row = sink_logit[layer].reshape(local_groups, per_group)
        attended = attend(
            queries.reshape(tokens, local_groups, per_group, HEAD_DIM),
            key_rows,
            value_all,
            sink_row,
            allowed,
        )
        attended = attended.reshape(tokens, local_heads * HEAD_DIM)

        def project():
            return lax.dot_general(
                attended, out_weight, (((1,), (1,)), ((), ())), preferred_element_type=jnp.float32
            )

        if layer < LAYERS - 1:
            share_rows = lax.psum_scatter(project(), "tp", scatter_dimension=0, tiled=True).astype(
                jnp.bfloat16
            )
            current = lax.all_gather(share_rows, "tp", axis=0, tiled=True)
        else:
            final_rows = lax.psum_scatter(
                project().astype(jnp.bfloat16), "tp", scatter_dimension=0, tiled=True
            )
    return norm_rows(final_rows, final_gain)


def solution(mesh):
    in_specs = (
        P("sp", None),
        P(),
        P(None, "sp", "tp"),
        P(None, "sp", "tp"),
        P(None, "sp", "tp"),
        P(None, "sp", "tp"),
        P(None, "tp"),
        P(),
    )
    out_specs = P(("sp", "tp"), None)
    return jax.shard_map(shards, mesh=mesh, in_specs=in_specs, out_specs=out_specs, check_vma=False)
```

profile of v0, /device:TPU:0, one launch (start us, length us, event | category | flops | bytes accessed | tf_op | source)
XLA Modules:
  0.0 580.5 jit_solution(9668719352871353835)
XLA Ops:
  19.5 37.0 %all-gather.7.cloned.1.call-done = bf16[3,2048,128]{2,1,0:T(8,128)(2,1)} async-done(((bf16[3,256,128]{2,1,0:T(8,128)(2,1)}), bf16[3,2048,128]{2,1,0:T(8,128)(2,1)}) %all-gather.7.cloned.1.call-update) | async-done | bytes 1572880 | tf_op jit(solution)/shard_map/all_gather | solution.py:83
  56.5 3.8 convolution_multiply_fusion.5
  60.4 40.8 %all-gather.9.cloned.1.call-done = bf16[3,2048,128]{2,1,0:T(8,128)(2,1)} async-done(((bf16[3,256,128]{2,1,0:T(8,128)(2,1)}), bf16[3,2048,128]{2,1,0:T(8,128)(2,1)}) %all-gather.9.cloned.1.call-update) | async-done | bytes 1572880 | tf_op jit(solution)/shard_map/all_gather | solution.py:84
  101.3 3.8 convolution_convert_fusion.3
  106.4 5.0 collective-permute-start
  114.4 48.1 %all-gather.11.cloned.1.call-done = bf16[3,2048,256]{2,1,0:T(8,128)(2,1)} async-done(((bf16[3,256,256]{2,1,0:T(8,128)(2,1)}), bf16[3,2048,256]{2,1,0:T(8,128)(2,1)}) %all-gather.11.cloned.1.call-update) | async-done | bytes 3145744 | tf_op jit(solution)/shard_map/all_gather | solution.py:82
  162.4 3.8 convolution_multiply_fusion.2
  170.2 4.7 fusion
  174.9 6.2 %fusion.24 = bf16[2,64,2,1024]{3,1,2,0:T(8,128)(2,1)S(1)} fusion(bf16[1280,2,64,1]{0,2,3,1:T(8,128)(2,1)S(1)} %bitcast.159, f32[2,1280,1024,2]{2,1,3,0:T(8,128)S(1)} %get-tuple-element.38, f32[2,2,1024]{2,1,0:T(2,128)S(1)} %exponential_add_fusion.2, f32[2,2,1024]{2,1,0:T(2,128)S(1)} %broadcast_maximum_fusion.2, pred[1024,1280]{0,1:T(8,128)(4,1)S(1)} %fusion.19), kind=kOutput, calls=%fused_computation.46 | convolution fusion | flops 697565184 | bytes 23166976 | tf_op jit(solution)/shard_map/kgqs,skd->qkgd/dot_general | solution.py:59
  181.1 42.1 %all-gather.13.cloned.1.call-done = bf16[3,2048,256]{2,1,0:T(8,128)(2,1)} async-done(((bf16[3,256,256]{2,1,0:T(8,128)(2,1)}), bf16[3,2048,256]{2,1,0:T(8,128)(2,1)}) %all-gather.13.cloned.1.call-update) | async-done | bytes 3145744 | tf_op jit(solution)/shard_map/all_gather | solution.py:85
  223.2 5.8 fusion.26
  229.1 70.2 %reduce-scatter.4.cloned.1.call-done = f32[256,2048]{1,0:T(8,128)} async-done(((f32[1024,2048]{1,0:T(8,128)}), f32[256,2048]{1,0:T(8,128)}) %reduce-scatter.4.cloned.1.call-update) | async-done | bytes 2097168 | tf_op jit(solution)/shard_map/reduce_scatter | solution.py:123
  302.3 34.3 %all-gather.15.cloned.1.call-done = bf16[1024,2048]{1,0:T(8,128)(2,1)} async-done(((bf16[256,2048]{1,0:T(8,128)(2,1)}), bf16[1024,2048]{1,0:T(8,128)(2,1)}) %all-gather.15.cloned.1.call-update) | async-done | bytes 4194320 | tf_op jit(solution)/shard_map/all_gather | solution.py:126
  346.8 4.5 collective-permute-start.2
  358.7 4.7 fusion.1
  363.4 7.8 %fusion.23 = bf16[2,64,2,1024]{3,1,2,0:T(8,128)(2,1)} fusion(bf16[1280,2,64,1]{0,2,3,1:T(8,128)(2,1)} %bitcast.161, f32[2,1280,1024,2]{2,1,3,0:T(8,128)S(1)} %get-tuple-element.40, f32[2,2,1024]{2,1,0:T(2,128)S(1)} %exponential_add_fusion.1, f32[2,2,1024]{2,1,0:T(2,128)S(1)} %broadcast_maximum_fusion.1, pred[1024,1280]{0,1:T(8,128)(4,1)S(1)} %fusion.19), kind=kOutput, calls=%fused_computation.45 | convolution fusion | flops 697565184 | bytes 23166976 | tf_op jit(solution)/shard_map/kgqs,skd->qkgd/dot_general | solution.py:59
  371.2 5.9 %fusion.25 = f32[1024,2048]{1,0:T(8,128)} fusion(bf16[1024,256]{0,1:T(8,128)(2,1)} %bitcast.158, bf16[3,2048,256]{2,1,0:T(8,128)(2,1)} %all-gather.13.cloned.1.call-done), kind=kOutput, calls=%fused_computation.56 | convolution fusion | flops 1073741824 | bytes 9961472 | tf_op jit(solution)/shard_map/dot_general | solution.py:118
  377.2 72.4 %reduce-scatter.6.cloned.1.call-done = f32[256,2048]{1,0:T(8,128)} async-done(((f32[1024,2048]{1,0:T(8,128)}), f32[256,2048]{1,0:T(8,128)}) %reduce-scatter.6.cloned.1.call-update) | async-done | bytes 2097168 | tf_op jit(solution)/shard_map/reduce_scatter | solution.py:123
  452.7 34.3 %all-gather.17.cloned.1.call-done = bf16[1024,2048]{1,0:T(8,128)(2,1)} async-done(((bf16[256,2048]{1,0:T(8,128)(2,1)}), bf16[1024,2048]{1,0:T(8,128)(2,1)}) %all-gather.17.cloned.1.call-update) | async-done | bytes 4194320 | tf_op jit(solution)/shard_map/all_gather | solution.py:126
  497.0 4.5 collective-permute-start.4
  508.2 4.7 fusion.2
  513.0 6.2 %fusion.22 = bf16[2,64,2,1024]{3,1,2,0:T(8,128)(2,1)S(1)} fusion(bf16[1280,2,64,1]{0,2,3,1:T(8,128)(2,1)S(1)} %bitcast.160, f32[2,1280,1024,2]{2,1,3,0:T(8,128)S(1)} %get-tuple-element.42, f32[2,2,1024]{2,1,0:T(2,128)S(1)} %exponential_add_fusion, f32[2,2,1024]{2,1,0:T(2,128)S(1)} %broadcast_maximum_fusion, pred[1024,1280]{0,1:T(8,128)(4,1)S(1)} %fusion.19), kind=kOutput, calls=%fused_computation.44 | convolution fusion | flops 697565184 | bytes 23166976 | tf_op jit(solution)/shard_map/kgqs,skd->qkgd/dot_general | solution.py:59
  519.2 4.5 convolution_convert_fusion
  523.7 45.7 %reduce-scatter.8.cloned.1.call-done = bf16[256,2048]{1,0:T(8,128)(2,1)} async-done(((bf16[1024,2048]{1,0:T(8,128)(2,1)}), bf16[256,2048]{1,0:T(8,128)(2,1)}) %reduce-scatter.8.cloned.1.call-update) | async-done | bytes 1048592 | tf_op jit(solution)/shard_map/reduce_scatter | solution.py:128
  (97 shorter events, 65.9 us)
Async XLA Ops:
  6.5 50.0 %all-gather.7.cloned.1.call-start = ((), (), s32[]{:S(2)}) async-start(), calls=%async_computation.3 | async-start | bytes 1769472 | tf_op jit(solution)/shard_map/all_gather | solution.py:83
  7.3 94.0 %all-gather.9.cloned.1.call-start = ((), (), s32[]{:S(2)}) async-start(), calls=%async_computation.4 | async-start | bytes 1769472 | tf_op jit(solution)/shard_map/all_gather | solution.py:84
  8.0 154.4 %all-gather.11.cloned.1.call-start = ((), (), s32[]{:S(2)}) async-start(), calls=%async_computation.5 | async-start | bytes 3538944 | tf_op jit(solution)/shard_map/all_gather | solution.py:82
  8.7 214.5 %all-gather.13.cloned.1.call-start = ((), (), s32[]{:S(2)}) async-start(), calls=%async_computation.6 | async-start | bytes 3538944 | tf_op jit(solution)/shard_map/all_gather | solution.py:85
  9.3 289.9 %reduce-scatter.4.cloned.1.call-start = ((), (), s32[]{:S(2)}) async-start(), calls=%async_computation.7 | async-start | bytes 10485760 | tf_op jit(solution)/shard_map/reduce_scatter | solution.py:123
  9.4 4.4 copy-start
  19.5 91.9 %copy-start.5 = (f32[3,4]{1,0:T(4,128)S(1)}, f32[3,4]{1,0:T(4,128)}, u32[]{:S(2)}) copy-start(f32[3,4]{1,0:T(4,128)} %param.14) | copy-start | bytes 148
  105.1 6.4 %collective-permute-start.1 = (bf16[128,256]{0,1:T(8,128)(2,1)S(1)}, bf16[128,256]{0,1:T(8,128)(2,1)S(1)}, u32[]{:S(2)}, u32[]{:S(2)}) collective-permute-start(bf16[128,256]{0,1:T(8,128)(2,1)S(1)} %get-tuple-element.31), channel_id=1, source_target_pairs={{4,0},{8,4},{12,8},{16,12},{20,16},{24,20},{28,24},{5,1},{9,5},{13... | collective-permute-start | bytes 196616 | tf_op jit(solution)/shard_map/ppermute | solution.py:21
  106.4 7.8 %collective-permute-start = (bf16[128,256]{0,1:T(8,128)(2,1)S(1)}, bf16[128,256]{0,1:T(8,128)(2,1)S(1)}, u32[]{:S(2)}, u32[]{:S(2)}) collective-permute-start(bf16[128,256]{0,1:T(8,128)(2,1)S(1)} %get-tuple-element.30), channel_id=1, source_target_pairs={{0,4},{4,8},{8,12},{12,16},{16,20},{20,24},{24,28},{1,5},{5,9},{9,... | collective-permute-start | bytes 196616 | tf_op jit(solution)/shard_map/ppermute | solution.py:18
  229.0 107.6 %all-gather.15.cloned.1.call-start = ((), (), s32[]{:S(2)}) async-start(), calls=%async_computation.8 | async-start | bytes 5242880 | tf_op jit(solution)/shard_map/all_gather | solution.py:126
  302.0 147.7 %reduce-scatter.6.cloned.1.call-start = ((), (), s32[]{:S(2)}) async-start(), calls=%async_computation.9 | async-start | bytes 10485760 | tf_op jit(solution)/shard_map/reduce_scatter | solution.py:123
  336.6 3.4 copy-start.2
  341.1 2.8 copy-start.3
  345.5 8.6 %collective-permute-start.3 = (bf16[128,256]{0,1:T(8,128)(2,1)S(1)}, bf16[128,256]{0,1:T(8,128)(2,1)S(1)}, u32[]{:S(2)}, u32[]{:S(2)}) collective-permute-start(bf16[128,256]{0,1:T(8,128)(2,1)S(1)} %get-tuple-element.29), channel_id=1, source_target_pairs={{4,0},{8,4},{12,8},{16,12},{20,16},{24,20},{28,24},{5,1},{9,5},{13... | collective-permute-start | bytes 196616 | tf_op jit(solution)/shard_map/ppermute | solution.py:21
  346.8 7.3 %collective-permute-start.2 = (bf16[128,256]{0,1:T(8,128)(2,1)S(1)}, bf16[128,256]{0,1:T(8,128)(2,1)S(1)}, u32[]{:S(2)}, u32[]{:S(2)}) collective-permute-start(bf16[128,256]{0,1:T(8,128)(2,1)S(1)} %get-tuple-element.28), channel_id=1, source_target_pairs={{0,4},{4,8},{8,12},{12,16},{16,20},{20,24},{24,28},{1,5},{5,9},{9,... | collective-permute-start | bytes 196616 | tf_op jit(solution)/shard_map/ppermute | solution.py:18
  377.2 109.8 %all-gather.17.cloned.1.call-start = ((), (), s32[]{:S(2)}) async-start(), calls=%async_computation.10 | async-start | bytes 5242880 | tf_op jit(solution)/shard_map/all_gather | solution.py:126
  452.4 117.0 %reduce-scatter.8.cloned.1.call-start = ((), (), s32[]{:S(2)}) async-start(), calls=%async_computation.11 | async-start | bytes 5242880 | tf_op jit(solution)/shard_map/reduce_scatter | solution.py:128
  487.0 3.4 copy-start.1
  495.7 8.6 %collective-permute-start.5 = (bf16[128,256]{0,1:T(8,128)(2,1)S(1)}, bf16[128,256]{0,1:T(8,128)(2,1)S(1)}, u32[]{:S(2)}, u32[]{:S(2)}) collective-permute-start(bf16[128,256]{0,1:T(8,128)(2,1)S(1)} %get-tuple-element.27), channel_id=1, source_target_pairs={{4,0},{8,4},{12,8},{16,12},{20,16},{24,20},{28,24},{5,1},{9,5},{13... | collective-permute-start | bytes 196616 | tf_op jit(solution)/shard_map/ppermute | solution.py:21
  497.0 7.3 %collective-permute-start.4 = (bf16[128,256]{0,1:T(8,128)(2,1)S(1)}, bf16[128,256]{0,1:T(8,128)(2,1)S(1)}, u32[]{:S(2)}, u32[]{:S(2)}) collective-permute-start(bf16[128,256]{0,1:T(8,128)(2,1)S(1)} %get-tuple-element.26), channel_id=1, source_target_pairs={{0,4},{4,8},{8,12},{12,16},{16,20},{20,24},{24,28},{1,5},{5,9},{9,... | collective-permute-start | bytes 196616 | tf_op jit(solution)/shard_map/ppermute | solution.py:18
  519.2 51.7 %copy-start.4 = (f32[2048]{0:T(1024)S(1)}, f32[2048]{0:T(1024)}, u32[]{:S(2)}) copy-start(f32[2048]{0:T(1024)} %param.15) | copy-start | bytes 24580
Sparse Core Ops, SparseCore 0:
  9.5 46.9 all-gather.6
  58.7 42.5 all-gather.8
  103.5 58.9 all-gather.10
  164.5 58.7 all-gather.12
  229.2 70.0 reduce-scatter.3
  302.1 34.4 all-gather.14
  377.3 72.3 reduce-scatter.5
  452.5 34.4 all-gather.16
  523.9 45.4 reduce-scatter.7
where the time goes:
time: 586 us; the launch traced here: 581 us
  waiting for transfers between devices  430 us (73%)
  matrix products  72.3 us (12%)
  other arithmetic  42.9 us (7%)
  starting transfers between devices  18.7 us (3%)
  between operations  13.9 us (2%)
    reduce_scatter x2, waiting for transfers between devices, shards(): lax.psum_scatter(project(), 'tp', scatter_dimension=0, tiled=True)  143 us
    all_gather x2, waiting for transfers between devices, shards(): current = lax.all_gather(share_rows, 'tp', axis=0, tiled=True)  68.6 us
    all_gather x1, waiting for transfers between devices, shards(): lax.all_gather(query_weight, 'sp', axis=1, tiled=True)  48.1 us
    reduce_scatter x1, waiting for transfers between devices, shards(): lax.psum_scatter(project().astype(jnp.bfloat16), 'tp', scatter_dimension=...  45.7 us
    all_gather x1, waiting for transfers between devices, shards(): lax.all_gather(output_weight, 'sp', axis=1, tiled=True)  42.1 us
    all_gather x1, waiting for transfers between devices, shards(): lax.all_gather(value_weight, 'sp', axis=1, tiled=True)  40.8 us
    all_gather x1, waiting for transfers between devices, shards(): lax.all_gather(key_weight, 'sp', axis=1, tiled=True)  37 us
    dot_general x3, matrix products, attend(): jnp.einsum('kgqs,skd->qkgd', weights, value_rows, preferred_element_type=...  20.2 us
  transfers between devices with their start and end apart: 15, of which 10 were waited for; matrix products, arithmetic and copies ran while one was open for 7% of the time, Pallas kernels for 0%

commit v1 on v0

--- a/solution.py
+++ b/solution.py
@@ -123,7 +123,16 @@
             share_rows = lax.psum_scatter(project(), "tp", scatter_dimension=0, tiled=True).astype(
                 jnp.bfloat16
             )
-            current = lax.all_gather(share_rows, "tp", axis=0, tiled=True)
+            ring = [share_rows]
+            for hop in range(3):
+                ring.append(
+                    lax.ppermute(ring[-1], "tp", [(dev, (dev + 1) % 4) for dev in range(4)])
+                )
+            current = jnp.roll(
+                jnp.concatenate(ring[::-1], axis=0),
+                (lax.axis_index("tp") + 1) * ring[0].shape[0],
+                axis=0,
+            )
         else:
             final_rows = lax.psum_scatter(
                 project().astype(jnp.bfloat16), "tp", scatter_dimension=0, tiled=True

time: 586 us -> 613 us (1.046)
  waiting for transfers between devices: 430 us -> 446 us
  other arithmetic: 42.9 us -> 53.4 us
    ppermute x0 -> x6, waiting for transfers between devices: none -> 85.9 us  [shards(): lax.ppermute(ring[-1], 'tp', [(dev, (dev + 1) % 4) for dev in range(4)])]
    all_gather x2 -> x0, waiting for transfers between devices: 68.6 us -> none  [shards(): current = lax.all_gather(share_rows, 'tp', axis=0, tiled=True)]
    reduce_sum x4, other arithmetic: 11.3 us -> 21.6 us  [norm_rows(): jnp.mean(wide_values * wide_values, axis=-1, keepdims=True) + EPS]
  transfers between devices with their start and end apart: 15 -> 19, of which waited for: 10 -> 14; matrix products, arithmetic and copies ran while one was open for 7% -> 7% of each run, Pallas kernels for 0% -> 0%
where the time goes in v1:
time: 613 us; the launch traced here: 608 us
  waiting for transfers between devices  446 us (73%)
  matrix products  72.5 us (12%)
  other arithmetic  53.4 us (9%)
  starting transfers between devices  18.7 us (3%)
  between operations  14.3 us (2%)
    reduce_scatter x2, waiting for transfers between devices, shards(): lax.psum_scatter(project(), 'tp', scatter_dimension=0, tiled=True)  143 us
    ppermute x6, waiting for transfers between devices, shards(): lax.ppermute(ring[-1], 'tp', [(dev, (dev + 1) % 4) for dev in range(4)])  85.9 us
    all_gather x1, waiting for transfers between devices, shards(): lax.all_gather(query_weight, 'sp', axis=1, tiled=True)  48.1 us
    reduce_scatter x1, waiting for transfers between devices, shards(): lax.psum_scatter(project().astype(jnp.bfloat16), 'tp', scatter_dimension=...  45.7 us
    all_gather x1, waiting for transfers between devices, shards(): lax.all_gather(output_weight, 'sp', axis=1, tiled=True)  42.1 us
    all_gather x1, waiting for transfers between devices, shards(): lax.all_gather(value_weight, 'sp', axis=1, tiled=True)  40.8 us
    all_gather x1, waiting for transfers between devices, shards(): lax.all_gather(key_weight, 'sp', axis=1, tiled=True)  35.1 us
    reduce_sum x4, other arithmetic, norm_rows(): jnp.mean(wide_values * wide_values, axis=-1, keepdims=True) + EPS  21.6 us
  transfers between devices with their start and end apart: 19, of which 14 were waited for; matrix products, arithmetic and copies ran while one was open for 7% of the time, Pallas kernels for 0%

profile of v1, /device:TPU:0, one launch (start us, length us, event | category | flops | bytes accessed | tf_op | source)
XLA Modules:
  0.0 607.8 jit_solution(10370509634117768333)
XLA Ops:
  13.4 5.2 fusion.11
  21.4 35.1 %all-gather.5.cloned.1.call-done = bf16[3,2048,128]{2,1,0:T(8,128)(2,1)} async-done(((bf16[3,256,128]{2,1,0:T(8,128)(2,1)}), bf16[3,2048,128]{2,1,0:T(8,128)(2,1)}) %all-gather.5.cloned.1.call-update) | async-done | bytes 1572880 | tf_op jit(solution)/shard_map/all_gather | solution.py:83
  60.4 40.8 %all-gather.7.cloned.1.call-done = bf16[3,2048,128]{2,1,0:T(8,128)(2,1)} async-done(((bf16[3,256,128]{2,1,0:T(8,128)(2,1)}), bf16[3,2048,128]{2,1,0:T(8,128)(2,1)}) %all-gather.7.cloned.1.call-update) | async-done | bytes 1572880 | tf_op jit(solution)/shard_map/all_gather | solution.py:84
  106.4 5.0 collective-permute-start
  114.3 48.1 %all-gather.9.cloned.1.call-done = bf16[3,2048,256]{2,1,0:T(8,128)(2,1)} async-done(((bf16[3,256,256]{2,1,0:T(8,128)(2,1)}), bf16[3,2048,256]{2,1,0:T(8,128)(2,1)}) %all-gather.9.cloned.1.call-update) | async-done | bytes 3145744 | tf_op jit(solution)/shard_map/all_gather | solution.py:82
  170.1 4.7 fusion
  174.9 6.2 %fusion.38 = bf16[2,64,2,1024]{3,1,2,0:T(8,128)(2,1)S(1)} fusion(bf16[1280,2,64,1]{0,2,3,1:T(8,128)(2,1)S(1)} %bitcast.159, f32[2,1280,1024,2]{2,1,3,0:T(8,128)S(1)} %get-tuple-element.43, f32[2,2,1024]{2,1,0:T(2,128)S(1)} %exponential_add_fusion.2, f32[2,2,1024]{2,1,0:T(2,128)S(1)} %broadcast_maximum_fusion.2, pred[1024,1280]{0,1:T(8,128)(4,1)S(1)} %fusion.19), kind=kOutput, calls=%fused_computation.76 | convolution fusion | flops 697565184 | bytes 23166976 | tf_op jit(solution)/shard_map/kgqs,skd->qkgd/dot_general | solution.py:59
  181.1 42.1 %all-gather.11.cloned.1.call-done = bf16[3,2048,256]{2,1,0:T(8,128)(2,1)} async-done(((bf16[3,256,256]{2,1,0:T(8,128)(2,1)}), bf16[3,2048,256]{2,1,0:T(8,128)(2,1)}) %all-gather.11.cloned.1.call-update) | async-done | bytes 3145744 | tf_op jit(solution)/shard_map/all_gather | solution.py:85
  223.2 5.8 fusion.40
  229.0 70.2 %reduce-scatter.4.cloned.1.call-done = f32[256,2048]{1,0:T(8,128)} async-done(((f32[1024,2048]{1,0:T(8,128)}), f32[256,2048]{1,0:T(8,128)}) %reduce-scatter.4.cloned.1.call-update) | async-done | bytes 2097168 | tf_op jit(solution)/shard_map/reduce_scatter | solution.py:123
  301.0 14.2 %collective-permute-done.2 = bf16[256,2048]{1,0:T(8,128)(2,1)S(1)} collective-permute-done((bf16[256,2048]{1,0:T(8,128)(2,1)S(1)}, bf16[256,2048]{1,0:T(8,128)(2,1)S(1)}, u32[]{:S(2)}, u32[]{:S(2)}) %collective-permute-start.2) | collective-permute-done | bytes 1048608 | tf_op jit(solution)/shard_map/ppermute | solution.py:129
  316.2 14.3 %collective-permute-done.3 = bf16[256,2048]{1,0:T(8,128)(2,1)} collective-permute-done((bf16[256,2048]{1,0:T(8,128)(2,1)S(1)}, bf16[256,2048]{1,0:T(8,128)(2,1)}, u32[]{:S(2)}, u32[]{:S(2)}) %collective-permute-start.3) | collective-permute-done | bytes 1048608 | tf_op jit(solution)/shard_map/ppermute | solution.py:129
  330.8 14.4 %collective-permute-done.4 = bf16[256,2048]{1,0:T(8,128)(2,1)} collective-permute-done((bf16[256,2048]{1,0:T(8,128)(2,1)}, bf16[256,2048]{1,0:T(8,128)(2,1)}, u32[]{:S(2)}, u32[]{:S(2)}) %collective-permute-start.4) | collective-permute-done | bytes 1048608 | tf_op jit(solution)/shard_map/ppermute | solution.py:129
  345.2 8.5 %fusion.12 = (f32[1024]{0:T(1024)S(1)}, bf16[1024,2048]{1,0:T(8,128)(2,1)S(1)}) fusion(s32[]{:T(128)S(6)} %select_n.26, bf16[256,2048]{1,0:T(8,128)(2,1)S(1)} %convert_element_type.115, bf16[256,2048]{1,0:T(8,128)(2,1)} %copy-done, bf16[256,2048]{1,0:T(8,128)(2,1)} %collective-permute-done.3, bf16[256,2048]{1,0:T(8,128)(2,1)} %collective-permute-done.4), kind=kLoop, calls=%fused_computation.27 | loop fusion | flops 39844864 | bytes 8392708 | tf_op jit(solution)/shard_map/reduce_sum | solution.py:28
  377.3 6.2 %fusion.37 = bf16[2,64,2,1024]{3,1,2,0:T(8,128)(2,1)S(1)} fusion(bf16[1280,2,64,1]{0,2,3,1:T(8,128)(2,1)S(1)} %bitcast.161, f32[2,1280,1024,2]{2,1,3,0:T(8,128)S(1)} %get-tuple-element.45, f32[2,2,1024]{2,1,0:T(2,128)S(1)} %exponential_add_fusion.1, f32[2,2,1024]{2,1,0:T(2,128)S(1)} %broadcast_maximum_fusion.1, pred[1024,1280]{0,1:T(8,128)(4,1)S(1)} %fusion.19), kind=kOutput, calls=%fused_computation.75 | convolution fusion | flops 697565184 | bytes 23166976 | tf_op jit(solution)/shard_map/kgqs,skd->qkgd/dot_general | solution.py:59
  383.5 5.8 fusion.39
  389.4 72.4 %reduce-scatter.6.cloned.1.call-done = f32[256,2048]{1,0:T(8,128)} async-done(((f32[1024,2048]{1,0:T(8,128)}), f32[256,2048]{1,0:T(8,128)}) %reduce-scatter.6.cloned.1.call-update) | async-done | bytes 2097168 | tf_op jit(solution)/shard_map/reduce_scatter | solution.py:123
  463.6 14.2 %collective-permute-done.7 = bf16[256,2048]{1,0:T(8,128)(2,1)S(1)} collective-permute-done((bf16[256,2048]{1,0:T(8,128)(2,1)S(1)}, bf16[256,2048]{1,0:T(8,128)(2,1)S(1)}, u32[]{:S(2)}, u32[]{:S(2)}) %collective-permute-start.7) | collective-permute-done | bytes 1048608 | tf_op jit(solution)/shard_map/ppermute | solution.py:129
  478.8 14.3 %collective-permute-done.8 = bf16[256,2048]{1,0:T(8,128)(2,1)} collective-permute-done((bf16[256,2048]{1,0:T(8,128)(2,1)S(1)}, bf16[256,2048]{1,0:T(8,128)(2,1)}, u32[]{:S(2)}, u32[]{:S(2)}) %collective-permute-start.8) | collective-permute-done | bytes 1048608 | tf_op jit(solution)/shard_map/ppermute | solution.py:129
  493.4 14.4 %collective-permute-done.9 = bf16[256,2048]{1,0:T(8,128)(2,1)} collective-permute-done((bf16[256,2048]{1,0:T(8,128)(2,1)}, bf16[256,2048]{1,0:T(8,128)(2,1)}, u32[]{:S(2)}, u32[]{:S(2)}) %collective-permute-start.9) | collective-permute-done | bytes 1048608 | tf_op jit(solution)/shard_map/ppermute | solution.py:129
  507.8 8.5 %fusion.15 = (f32[1024]{0:T(1024)S(1)}, bf16[1024,2048]{1,0:T(8,128)(2,1)S(1)}) fusion(s32[]{:T(128)S(6)} %select_n.26, bf16[256,2048]{1,0:T(8,128)(2,1)S(1)} %convert_element_type.123, bf16[256,2048]{1,0:T(8,128)(2,1)} %copy-done.1, bf16[256,2048]{1,0:T(8,128)(2,1)} %collective-permute-done.8, bf16[256,2048]{1,0:T(8,128)(2,1)} %collective-permute-done.9), kind=kLoop, calls=%fused_computation.30 | loop fusion | flops 39844864 | bytes 8392708 | tf_op jit(solution)/shard_map/reduce_sum | solution.py:28
  535.2 4.7 fusion.2
  540.0 6.2 %fusion.36 = bf16[2,64,2,1024]{3,1,2,0:T(8,128)(2,1)S(1)} fusion(bf16[1280,2,64,1]{0,2,3,1:T(8,128)(2,1)S(1)} %bitcast.160, f32[2,1280,1024,2]{2,1,3,0:T(8,128)S(1)} %get-tuple-element.47, f32[2,2,1024]{2,1,0:T(2,128)S(1)} %exponential_add_fusion, f32[2,2,1024]{2,1,0:T(2,128)S(1)} %broadcast_maximum_fusion, pred[1024,1280]{0,1:T(8,128)(4,1)S(1)} %fusion.19), kind=kOutput, calls=%fused_computation.74 | convolution fusion | flops 697565184 | bytes 23166976 | tf_op jit(solution)/shard_map/kgqs,skd->qkgd/dot_general | solution.py:59
  550.7 45.7 %reduce-scatter.8.cloned.1.call-done = bf16[256,2048]{1,0:T(8,128)(2,1)} async-done(((bf16[1024,2048]{1,0:T(8,128)(2,1)}), bf16[256,2048]{1,0:T(8,128)(2,1)}) %reduce-scatter.8.cloned.1.call-update) | async-done | bytes 1048592 | tf_op jit(solution)/shard_map/reduce_scatter | solution.py:137
  (99 shorter events, 86.5 us)
Async XLA Ops:
  6.5 49.9 %all-gather.5.cloned.1.call-start = ((), (), s32[]{:S(2)}) async-start(), calls=%async_computation.3 | async-start | bytes 1769472 | tf_op jit(solution)/shard_map/all_gather | solution.py:83
  7.3 94.0 %all-gather.7.cloned.1.call-start = ((), (), s32[]{:S(2)}) async-start(), calls=%async_computation.4 | async-start | bytes 1769472 | tf_op jit(solution)/shard_map/all_gather | solution.py:84
  8.0 154.4 %all-gather.9.cloned.1.call-start = ((), (), s32[]{:S(2)}) async-start(), calls=%async_computation.5 | async-start | bytes 3538944 | tf_op jit(solution)/shard_map/all_gather | solution.py:82
  8.7 214.5 %all-gather.11.cloned.1.call-start = ((), (), s32[]{:S(2)}) async-start(), calls=%async_computation.6 | async-start | bytes 3538944 | tf_op jit(solution)/shard_map/all_gather | solution.py:85
  9.3 289.9 %reduce-scatter.4.cloned.1.call-start = ((), (), s32[]{:S(2)}) async-start(), calls=%async_computation.7 | async-start | bytes 10485760 | tf_op jit(solution)/shard_map/reduce_scatter | solution.py:123
  18.6 92.8 %copy-start.3 = (f32[3,4]{1,0:T(4,128)S(1)}, f32[3,4]{1,0:T(4,128)}, u32[]{:S(2)}) copy-start(f32[3,4]{1,0:T(4,128)} %param.16) | copy-start | bytes 148
  105.1 6.4 %collective-permute-start.1 = (bf16[128,256]{0,1:T(8,128)(2,1)S(1)}, bf16[128,256]{0,1:T(8,128)(2,1)S(1)}, u32[]{:S(2)}, u32[]{:S(2)}) collective-permute-start(bf16[128,256]{0,1:T(8,128)(2,1)S(1)} %get-tuple-element.36), channel_id=1, source_target_pairs={{4,0},{8,4},{12,8},{16,12},{20,16},{24,20},{28,24},{5,1},{9,5},{13... | collective-permute-start | bytes 196616 | tf_op jit(solution)/shard_map/ppermute | solution.py:21
  106.4 7.8 %collective-permute-start = (bf16[128,256]{0,1:T(8,128)(2,1)S(1)}, bf16[128,256]{0,1:T(8,128)(2,1)S(1)}, u32[]{:S(2)}, u32[]{:S(2)}) collective-permute-start(bf16[128,256]{0,1:T(8,128)(2,1)S(1)} %get-tuple-element.35), channel_id=1, source_target_pairs={{0,4},{4,8},{8,12},{12,16},{16,20},{20,24},{24,28},{1,5},{5,9},{9,... | collective-permute-start | bytes 196616 | tf_op jit(solution)/shard_map/ppermute | solution.py:18
  229.0 232.8 %reduce-scatter.6.cloned.1.call-start = ((), (), s32[]{:S(2)}) async-start(), calls=%async_computation.8 | async-start | bytes 10485760 | tf_op jit(solution)/shard_map/reduce_scatter | solution.py:123
  300.9 14.3 %collective-permute-start.2 = (bf16[256,2048]{1,0:T(8,128)(2,1)S(1)}, bf16[256,2048]{1,0:T(8,128)(2,1)S(1)}, u32[]{:S(2)}, u32[]{:S(2)}) collective-permute-start(bf16[256,2048]{1,0:T(8,128)(2,1)S(1)} %convert_element_type.115), channel_id=1, source_target_pairs={{0,1},{1,2},{2,3},{3,0},{4,5},{5,6},{6,7},{7,4},{8,9},{9,10},{10,1... | collective-permute-start | bytes 3145736 | tf_op jit(solution)/shard_map/ppermute | solution.py:129
  315.2 1.0 copy-start
  316.2 14.3 %collective-permute-start.3 = (bf16[256,2048]{1,0:T(8,128)(2,1)S(1)}, bf16[256,2048]{1,0:T(8,128)(2,1)}, u32[]{:S(2)}, u32[]{:S(2)}) collective-permute-start(bf16[256,2048]{1,0:T(8,128)(2,1)S(1)} %collective-permute-done.2), channel_id=1, source_target_pairs={{0,1},{1,2},{2,3},{3,0},{4,5},{5,6},{6,7},{7,4},{8,9},{9,10},{10,1... | collective-permute-start | bytes 3145736 | tf_op jit(solution)/shard_map/ppermute | solution.py:129
  330.5 14.7 %collective-permute-start.4 = (bf16[256,2048]{1,0:T(8,128)(2,1)}, bf16[256,2048]{1,0:T(8,128)(2,1)}, u32[]{:S(2)}, u32[]{:S(2)}) collective-permute-start(bf16[256,2048]{1,0:T(8,128)(2,1)} %collective-permute-done.3), channel_id=1, source_target_pairs={{0,1},{1,2},{2,3},{3,0},{4,5},{5,6},{6,7},{7,4},{8,9},{9,10},{10,1... | collective-permute-start | bytes 3145736 | tf_op jit(solution)/shard_map/ppermute | solution.py:129
  360.0 8.6 %collective-permute-start.6 = (bf16[128,256]{0,1:T(8,128)(2,1)S(1)}, bf16[128,256]{0,1:T(8,128)(2,1)S(1)}, u32[]{:S(2)}, u32[]{:S(2)}) collective-permute-start(bf16[128,256]{0,1:T(8,128)(2,1)S(1)} %get-tuple-element.34), channel_id=1, source_target_pairs={{4,0},{8,4},{12,8},{16,12},{20,16},{24,20},{28,24},{5,1},{9,5},{13... | collective-permute-start | bytes 196616 | tf_op jit(solution)/shard_map/ppermute | solution.py:21
  361.3 7.3 %collective-permute-start.5 = (bf16[128,256]{0,1:T(8,128)(2,1)S(1)}, bf16[128,256]{0,1:T(8,128)(2,1)S(1)}, u32[]{:S(2)}, u32[]{:S(2)}) collective-permute-start(bf16[128,256]{0,1:T(8,128)(2,1)S(1)} %get-tuple-element.33), channel_id=1, source_target_pairs={{0,4},{4,8},{8,12},{12,16},{16,20},{20,24},{24,28},{1,5},{5,9},{9,... | collective-permute-start | bytes 196616 | tf_op jit(solution)/shard_map/ppermute | solution.py:18
  389.3 207.1 %reduce-scatter.8.cloned.1.call-start = ((), (), s32[]{:S(2)}) async-start(), calls=%async_computation.9 | async-start | bytes 5242880 | tf_op jit(solution)/shard_map/reduce_scatter | solution.py:137
  463.5 14.3 %collective-permute-start.7 = (bf16[256,2048]{1,0:T(8,128)(2,1)S(1)}, bf16[256,2048]{1,0:T(8,128)(2,1)S(1)}, u32[]{:S(2)}, u32[]{:S(2)}) collective-permute-start(bf16[256,2048]{1,0:T(8,128)(2,1)S(1)} %convert_element_type.123), channel_id=1, source_target_pairs={{0,1},{1,2},{2,3},{3,0},{4,5},{5,6},{6,7},{7,4},{8,9},{9,10},{10,1... | collective-permute-start | bytes 3145736 | tf_op jit(solution)/shard_map/ppermute | solution.py:129
  477.8 1.0 copy-start.1
  478.8 14.3 %collective-permute-start.8 = (bf16[256,2048]{1,0:T(8,128)(2,1)S(1)}, bf16[256,2048]{1,0:T(8,128)(2,1)}, u32[]{:S(2)}, u32[]{:S(2)}) collective-permute-start(bf16[256,2048]{1,0:T(8,128)(2,1)S(1)} %collective-permute-done.7), channel_id=1, source_target_pairs={{0,1},{1,2},{2,3},{3,0},{4,5},{5,6},{6,7},{7,4},{8,9},{9,10},{10,1... | collective-permute-start | bytes 3145736 | tf_op jit(solution)/shard_map/ppermute | solution.py:129
  493.1 14.7 %collective-permute-start.9 = (bf16[256,2048]{1,0:T(8,128)(2,1)}, bf16[256,2048]{1,0:T(8,128)(2,1)}, u32[]{:S(2)}, u32[]{:S(2)}) collective-permute-start(bf16[256,2048]{1,0:T(8,128)(2,1)} %collective-permute-done.8), channel_id=1, source_target_pairs={{0,1},{1,2},{2,3},{3,0},{4,5},{5,6},{6,7},{7,4},{8,9},{9,10},{10,1... | collective-permute-start | bytes 3145736 | tf_op jit(solution)/shard_map/ppermute | solution.py:129
  522.7 8.6 %collective-permute-start.11 = (bf16[128,256]{0,1:T(8,128)(2,1)S(1)}, bf16[128,256]{0,1:T(8,128)(2,1)S(1)}, u32[]{:S(2)}, u32[]{:S(2)}) collective-permute-start(bf16[128,256]{0,1:T(8,128)(2,1)S(1)} %get-tuple-element.32), channel_id=1, source_target_pairs={{4,0},{8,4},{12,8},{16,12},{20,16},{24,20},{28,24},{5,1},{9,5},{13... | collective-permute-start | bytes 196616 | tf_op jit(solution)/shard_map/ppermute | solution.py:21
  524.0 7.3 %collective-permute-start.10 = (bf16[128,256]{0,1:T(8,128)(2,1)S(1)}, bf16[128,256]{0,1:T(8,128)(2,1)S(1)}, u32[]{:S(2)}, u32[]{:S(2)}) collective-permute-start(bf16[128,256]{0,1:T(8,128)(2,1)S(1)} %get-tuple-element.31), channel_id=1, source_target_pairs={{0,4},{4,8},{8,12},{12,16},{16,20},{20,24},{24,28},{1,5},{5,9},{9,... | collective-permute-start | bytes 196616 | tf_op jit(solution)/shard_map/ppermute | solution.py:18
  546.2 51.7 %copy-start.2 = (f32[2048]{0:T(1024)S(1)}, f32[2048]{0:T(1024)}, u32[]{:S(2)}) copy-start(f32[2048]{0:T(1024)} %param.17) | copy-start | bytes 24580
Sparse Core Ops, SparseCore 0:
  9.5 46.9 all-gather.4
  58.6 42.5 all-gather.6
  103.4 58.9 all-gather.8
  164.4 58.7 all-gather.10
  229.1 70.0 reduce-scatter.3
  389.4 72.3 reduce-scatter.5
  550.8 45.5 reduce-scatter.7
